TPU v7x, 32 devices: a whole 2x2x4 slice. The times are simulated.
32 devices in a mesh: grp: 2 (over y), ep: 4 (over z), tp: 4 (over x, core).
Axes of the slice: x: 2, y: 2, z: 4, core: 2. Of those that a mesh axis runs over, the one named last changes fastest.
Arguments:
- query_first: bfloat16 [3072, 512], P(('grp', 'ep'), 'tp'), parts along dimension 0, may hold values from -32 to 32
- query_second: bfloat16 [3072, 512], P(('grp', 'ep'), 'tp'), parts along dimension 0, may hold values from -32 to 32
- key_first: bfloat16 [3072, 512], P(('grp', 'ep'), 'tp'), parts along dimension 0, may hold values from -32 to 32
- key_second: bfloat16 [3072, 512], P(('grp', 'ep'), 'tp'), parts along dimension 0, may hold values from -32 to 32
- values: bfloat16 [3072, 1024], P(('grp', 'ep'), 'tp'), parts along dimension 0, may hold values from -6 to 6
- lambda_head: float32 [8], P('tp'), may hold values from 0.3 to 0.8
- head_gain: float32 [128], replicated, may hold values from 0.1 to 1.9
- out_weight: bfloat16 [1024, 2048], replicated, may hold values from -0.1875 to 0.1875
- tokens: bfloat16 [4096, 2048], P(('grp', 'ep', 'tp')), parts along dimension 0, may hold values from -6 to 6
- norm_gain: float32 [2048], replicated, may hold values from 0.1 to 1.9
- expert_ids: int32 [4096, 2], P(('grp', 'ep', 'tp')), parts along dimension 0, may hold values from 0 to 3, all different within a row; in each aligned block of 128 rows (0 to 127, 128 to 255, ...) at most 96 rows name the same one
- expert_weights: float32 [4096, 2], P(('grp', 'ep', 'tp')), parts along dimension 0, may hold values from 0.2 to 1
- expert_gate: bfloat16 [4, 2048, 1024], P('ep', None, 'tp'), may hold values from -0.125 to 0.125
- expert_up: bfloat16 [4, 2048, 1024], P('ep', None, 'tp'), may hold values from -0.125 to 0.125
- expert_down: bfloat16 [4, 1024, 2048], P('ep', 'tp'), may hold values from -0.1875 to 0.1875
- shared_gate: bfloat16 [2048, 512], P(None, 'tp'), may hold values from -0.125 to 0.125
- shared_up: bfloat16 [2048, 512], P(None, 'tp'), may hold values from -0.125 to 0.125
- shared_down: bfloat16 [512, 2048], P('tp'), may hold values from -0.25 to 0.25
Outputs:
- mixed: bfloat16 [3072, 2048], P(('grp', 'ep', 'tp')), parts along dimension 0
- expert_out: bfloat16 [4096, 2048], P(('grp', 'ep', 'tp')), parts along dimension 0
There are 2 independent parts, one for each index of `grp`. A program takes and returns all parts, laid end to end along the dimension named above; an argument that names none is the same for every part. Nothing has to cross between parts.
Inputs may be any that keep to these rules, and one draw needn't show every extreme that they name: `expert_ids`: in the rows of one device (aligned blocks of 128 rows) no expert is named by more than 96 rows, and in every draw some expert is named by exactly 96 rows of some block; each row names 2 different experts.
All inputs are finite; a program needn't handle non-finite values.
Results may differ from a plain program's by a relative error of at most 0.012.
Values may be sent and summed in bfloat16 or wider, within the bound.
No kernel may reach another device: no remote copies, remote signals or barrier semaphores. Data moves between devices by JAX's collectives and lax.ppermute only.
A program may use at most 128 MiB of HBM per device.

v0:
```python
import jax
import jax.numpy as jnp
from jax import lax
from jax.sharding import PartitionSpec as P

epsilon = 1e-06
block_limit = 1536


def key_block(total_rows, shard_rows):
    if total_rows <= block_limit or total_rows % shard_rows != 0:
        return total_rows
    best_rows = shard_rows
    for factor_rows in range(1, total_rows // shard_rows + 1):
        if total_rows % (factor_rows * shard_rows) == 0 and factor_rows * shard_rows <= block_limit:
            best_rows = factor_rows * shard_rows
    return best_rows


def softmax_update(states, scores, value_block):
    running_max, running_sum, accumulated = states
    new_max = jnp.maximum(running_max, jnp.max(scores, axis=-1))
    rescale = jnp.exp(running_max - new_max)
    weights = jnp.exp(scores - new_max[..., None])
    new_sum = running_sum * rescale + jnp.sum(weights, axis=-1)
    product = jnp.einsum(
        "qhk,khe->qhe",
        weights.astype(jnp.bfloat16),
        value_block,
        preferred_element_type=jnp.float32,
    )
    return (new_max, new_sum, accumulated * rescale[..., None] + product)


def shards(
    query_first,
    query_second,
    key_first,
    key_second,
    values,
    lambda_head,
    head_gain,
    out_weight,
    tokens,
    norm_gain,
    expert_ids,
    expert_weights,
    expert_gate,
    expert_up,
    expert_down,
    shared_gate,
    shared_up,
    shared_down,
):
    shard_rows, query_width = query_first.shape
    heads_here = lambda_head.shape[0]
    head_size = query_width // heads_here
    value_size = values.shape[1] // heads_here
    score_scale = head_size ** (-0.5)
    query_one = query_first.reshape(shard_rows, heads_here, head_size)
    query_two = query_second.reshape(shard_rows, heads_here, head_size)
    initial = (
        jnp.full((shard_rows, heads_here), -jnp.inf, jnp.float32),
        jnp.zeros((shard_rows, heads_here), jnp.float32),
        jnp.zeros((shard_rows, heads_here, value_size), jnp.float32),
    )
    carried = (initial, initial)
    key_one = lax.all_gather(key_first, "ep", axis=0, tiled=True)
    key_two = lax.all_gather(key_second, "ep", axis=0, tiled=True)
    value_piece = lax.all_gather(values, "ep", axis=0, tiled=True)
    total_rows = key_one.shape[0]
    block_rows = key_block(total_rows, shard_rows)
    block_count = total_rows // block_rows
    stacked = (
        key_one.reshape(block_count, block_rows, heads_here, head_size),
        key_two.reshape(block_count, block_rows, heads_here, head_size),
        value_piece.reshape(block_count, block_rows, heads_here, value_size),
    )

    def fold_step(states, blocks):
        first_state, second_state = states
        key_a, key_b, value_block = blocks
        scores_a = (
            jnp.einsum("qhd,khd->qhk", query_one, key_a, preferred_element_type=jnp.float32)
            * score_scale
        )
        scores_b = (
            jnp.einsum("qhd,khd->qhk", query_two, key_b, preferred_element_type=jnp.float32)
            * score_scale
        )
        return (
            (
                softmax_update(first_state, scores_a, value_block),
                softmax_update(second_state, scores_b, value_block),
            ),
            None,
        )

    carried, unused = lax.scan(fold_step, carried, stacked)
    first_state, second_state = carried
    first_out = first_state[2] / first_state[1][..., None]
    second_out = second_state[2] / second_state[1][..., None]
    mixture = first_out - lambda_head[None, :, None] * second_out
    normed_heads = (
        mixture
        * lax.rsqrt(jnp.mean(mixture * mixture, axis=-1, keepdims=True) + epsilon)
        * head_gain
    )
    head_local = normed_heads.astype(jnp.bfloat16).reshape(shard_rows, heads_here * value_size)
    position_heads = lax.all_to_all(head_local, "tp", split_axis=0, concat_axis=1, tiled=True)
    mixed = jnp.dot(position_heads, out_weight, preferred_element_type=jnp.float32).astype(
        jnp.bfloat16
    )
    row_count, model_width = tokens.shape
    top_count = expert_ids.shape[1]
    ep_count = lax.axis_size("ep")
    local_experts = expert_gate.shape[0]
    expert_count = local_experts * ep_count
    capacity = max(2, row_count * top_count * 3 // (2 * expert_count))
    routed_rows = expert_count * capacity
    owner_span = routed_rows + row_count
    widened = tokens.astype(jnp.float32)
    normed = (
        widened
        * lax.rsqrt(jnp.mean(widened * widened, axis=-1, keepdims=True) + epsilon)
        * norm_gain
    ).astype(jnp.bfloat16)
    flat_ids = expert_ids.reshape(-1)
    onehot = (flat_ids[:, None] == jnp.arange(expert_count, dtype=jnp.int32)[None, :]).astype(
        jnp.int32
    )
    ranks = jnp.sum(onehot * jnp.cumsum(onehot, axis=0), axis=1) - 1
    slot_index = flat_ids * capacity + ranks
    token_index = jnp.arange(flat_ids.shape[0], dtype=jnp.int32) // top_count
    filled = jnp.full((routed_rows,), row_count, jnp.int32).at[slot_index].set(token_index)
    padded = jnp.concatenate([normed, jnp.zeros((1, model_width), jnp.bfloat16)], axis=0)
    outgoing = padded[filled].reshape(1, ep_count, local_experts * capacity, model_width)
    arrived = lax.all_to_all(outgoing, "ep", split_axis=1, concat_axis=1, tiled=True)
    local_rows = jnp.concatenate(
        [arrived.reshape(1, routed_rows, model_width), normed[None]], axis=1
    )
    gathered = lax.all_gather(local_rows, "tp", axis=0, tiled=True)
    owners = owner_span * lax.axis_size("tp") // owner_span
    routed_in = gathered[:, :routed_rows].reshape(
        owners, ep_count, local_experts, capacity, model_width
    )
    gate_value = jnp.einsum(
        "osecd,edf->osecf", routed_in, expert_gate, preferred_element_type=jnp.float32
    )
    up_value = jnp.einsum(
        "osecd,edf->osecf", routed_in, expert_up, preferred_element_type=jnp.float32
    )
    hidden = (jax.nn.silu(gate_value) * up_value).astype(jnp.bfloat16)
    routed_out = jnp.einsum(
        "osecf,efd->osecd", hidden, expert_down, preferred_element_type=jnp.float32
    )
    routed_out = routed_out.reshape(owners, routed_rows, model_width)
    shared_in = gathered[:, routed_rows:]
    shared_gate_value = jnp.einsum(
        "ord,df->orf", shared_in, shared_gate, preferred_element_type=jnp.float32
    )
    shared_up_value = jnp.einsum(
        "ord,df->orf", shared_in, shared_up, preferred_element_type=jnp.float32
    )
    shared_hidden = (jax.nn.silu(shared_gate_value) * shared_up_value).astype(jnp.bfloat16)
    shared_out = jnp.einsum(
        "orf,fd->ord", shared_hidden, shared_down, preferred_element_type=jnp.float32
    )
    kept_rows = lax.psum_scatter(
        jnp.concatenate([routed_out, shared_out], axis=1)
        .reshape(owners * owner_span, model_width)
        .astype(jnp.bfloat16),
        "tp",
        scatter_dimension=0,
        tiled=True,
    ).astype(jnp.float32)
    routed_back = (
        kept_rows[:routed_rows]
        .astype(jnp.bfloat16)
        .reshape(ep_count, local_experts * capacity, model_width)
    )
    returned = lax.all_to_all(routed_back, "ep", split_axis=0, concat_axis=0, tiled=True).reshape(
        routed_rows, model_width
    )
    picked = returned[slot_index].reshape(row_count, top_count, model_width).astype(jnp.float32)
    combined = jnp.sum(picked * expert_weights[:, :, None], axis=1) + kept_rows[routed_rows:]
    expert_out = combined.astype(jnp.bfloat16)
    return (mixed, expert_out)


def solution(mesh):
    placed = (
        P(("grp", "ep"), "tp"),
        P(("grp", "ep"), "tp"),
        P(("grp", "ep"), "tp"),
        P(("grp", "ep"), "tp"),
        P(("grp", "ep"), "tp"),
        P("tp"),
        P(),
        P(),
        P(("grp", "ep", "tp"), None),
        P(),
        P(("grp", "ep", "tp"), None),
        P(("grp", "ep", "tp"), None),
        P("ep", None, "tp"),
        P("ep", None, "tp"),
        P("ep", "tp", None),
        P(None, "tp"),
        P(None, "tp"),
        P("tp", None),
    )
    return jax.shard_map(
        shards,
        mesh=mesh,
        in_specs=placed,
        out_specs=(P(("grp", "ep", "tp"), None), P(("grp", "ep", "tp"), None)),
        check_vma=False,
    )
```

profile of v0, /device:TPU:0, one launch (start us, length us, event | category | flops | bytes accessed | tf_op | source)
XLA Modules:
  0.0 291.5 jit_solution(5120199368730788813)
XLA Ops:
  7.2 0.0 copy-start
  7.2 0.8 broadcast_multiply_fusion
  8.0 0.8 copy.55
  8.7 0.1 eq.29
  8.9 0.1 eq.25
  9.0 1.2 fusion.55
  10.3 0.1 copy.54
  10.4 0.1 mul.161
  10.5 1.2 reduce-window.6
  11.8 0.1 slice.33
  11.8 0.1 copy.57
  12.0 0.1 copy.58
  12.1 0.1 add_bitcast_fusion
  12.2 1.4 scatter_custom_fusion
  13.6 1.2 fusion.57
  14.9 0.0 copy-start.3
  14.9 0.0 copy-start.9
  14.9 3.1 %gather_fusion = bf16[384,2048]{1,0:T(8,128)(2,1)} fusion(bf16[129,2048]{1,0:T(8,128)(2,1)S(1)} %concatenate.10, s32[1024]{0:T(1024)S(1)} %pad_clamp_fusion.1), kind=kCustom, calls=%fused_computation | custom fusion | bytes 3147264 | tf_op jit(solution)/shard_map/gather | solution.py:137
  18.1 6.3 %all-to-all-start.1 = ((bf16[1,4,96,2048]{3,2,0,1:T(8,128)(2,1)}), bf16[1,4,96,2048]{3,2,0,1:T(8,128)(2,1)S(1)}, u32[]{:S(2)}, u32[]{:S(2)}) async-start(bf16[1,4,96,2048]{3,2,0,1:T(8,128)(2,1)} %bitcast.182), calls=%async_computation.1 | async-start | bytes 3145728 | tf_op jit(solution)/shard_map/all_to_all | solution.py:138
  24.4 1.0 fusion.94
  25.4 36.0 %all-to-all-done.1 = bf16[1,4,96,2048]{3,2,0,1:T(8,128)(2,1)S(1)} async-done(((bf16[1,4,96,2048]{3,2,0,1:T(8,128)(2,1)}), bf16[1,4,96,2048]{3,2,0,1:T(8,128)(2,1)S(1)}, u32[]{:S(2)}, u32[]{:S(2)}) %all-to-all-start.1) | async-done | bytes 1572896 | tf_op jit(solution)/shard_map/all_to_all | solution.py:138
  61.4 2.6 pad_maximum_fusion.1
  64.0 0.0 all-gather.2.cloned.1.call-update
  64.0 0.0 copy-start.12
  64.0 0.2 reduce-scatter.2.cloned.1.call-start
  64.2 57.3 %all-gather.2.cloned.1.call-done = bf16[4,512,2048]{2,1,0:T(8,128)(2,1)} async-done(((bf16[1,512,2048]{2,1,0:T(8,128)(2,1)}), bf16[4,512,2048]{2,1,0:T(8,128)(2,1)}) %all-gather.2.cloned.1.call-update) | async-done | bytes 8388624 | tf_op jit(solution)/shard_map/all_gather | solution.py:142
  121.5 3.4 %slice.34 = bf16[4,384,2048]{2,1,0:T(8,128)(2,1)S(1)} slice(bf16[4,512,2048]{2,1,0:T(8,128)(2,1)} %all-gather.2.cloned.1.call-done), slice={[0:4], [0:384], [0:2048]} | slice | bytes 12582912 | tf_op jit(solution)/shard_map/slice | solution.py:144
  124.9 2.6 copy-done.2
  127.5 3.0 %fusion.61 = f32[4,4,96,256]{3,2,1,0:T(8,128)} fusion(bf16[4,4,96,2048]{3,2,1,0:T(8,128)(2,1)S(1)} %bitcast.177, bf16[1,2048,256]{2,1,0:T(8,128)(2,1)S(1)} %copy-done.12), kind=kOutput, calls=%fused_computation.54 | convolution fusion | flops 1610612736 | bytes 8912896 | tf_op jit(solution)/shard_map/osecd,edf->osecf/dot_general | solution.py:147
  130.5 12.4 %convolution_convert_fusion = bf16[4,4,96,2048]{3,2,1,0:T(8,128)(2,1)} fusion(bf16[4,4,96,2048]{3,2,1,0:T(8,128)(2,1)} %bitcast.178, f32[4,4,96,256]{3,2,1,0:T(8,128)} %fusion.61, bf16[1,256,2048]{2,1,0:T(8,128)(2,1)S(1)} %copy-done, bf16[1,2048,256]{2,1,0:T(8,128)(2,1)S(1)} %copy-done.13), kind=kOutput, calls=%fused_computation.10 | convolution fusion | flops 3226730496 | bytes 16252928 | tf_op jit(solution)/shard_map/osecf,efd->osecd/dot_general | solution.py:154
  142.9 2.3 fusion.16
  145.2 4.1 %convolution_convert_fusion.1 = bf16[4,128,2048]{2,1,0:T(8,128)(2,1)S(1)} fusion(bf16[4,512,2048]{2,1,0:T(8,128)(2,1)} %all-gather.2.cloned.1.call-done, bf16[128,2048]{1,0:T(8,128)(2,1)} %param.35, bf16[2048,128]{1,0:T(8,128)(2,1)} %param.34, f32[4,128,128]{2,1,0:T(8,128)S(1)} %fusion.16), kind=kOutput, calls=%fused_computation.15 | convolution fusion | flops 538312704 | bytes 5505024 | tf_op jit(solution)/shard_map/orf,fd->ord/dot_general | solution.py:166
  149.4 7.6 %pad_maximum_fusion = bf16[4,512,2048]{2,1,0:T(8,128)(2,1)} fusion(bf16[4,128,2048]{2,1,0:T(8,128)(2,1)S(1)} %convolution_convert_fusion.1, bf16[4,384,2048]{2,1,0:T(8,128)(2,1)} %bitcast.181), kind=kLoop, calls=%fused_computation.3 | loop fusion | flops 16777216 | bytes 16777216 | tf_op jit(solution)/shard_map/concatenate | solution.py:170
  157.0 0.0 reduce-scatter.2.cloned.1.call-update
  157.0 0.9 copy-done.4
  157.9 19.7 %all_gather.13 = bf16[1536,256]{1,0:T(8,128)(2,1)S(1)} all-gather(bf16[384,256]{1,0:T(8,128)(2,1)S(1)} %copy-done.4), channel_id=1, replica_groups=mesh['grp'=2,'ep'=4,'tp'=4] {'ep'}, dimensions={0}, use_global_device_ids=true | all-gather | bytes 983040 | tf_op jit(solution)/shard_map/all_gather | solution.py:70
  177.6 0.3 copy.47
  177.9 15.2 %all_gather.14 = bf16[1536,128]{1,0:T(8,128)(2,1)S(1)} all-gather(bf16[384,128]{1,0:T(8,128)(2,1)S(1)} %copy-done.7), channel_id=1, replica_groups=mesh['grp'=2,'ep'=4,'tp'=4] {'ep'}, dimensions={0}, use_global_device_ids=true | all-gather | bytes 491520 | tf_op jit(solution)/shard_map/all_gather | solution.py:69
  193.1 0.2 copy.49
  193.3 0.1 copy.50
  193.5 15.1 %all_gather.12 = bf16[1536,128]{1,0:T(8,128)(2,1)S(1)} all-gather(bf16[384,128]{1,0:T(8,128)(2,1)S(1)} %copy-done.8), channel_id=1, replica_groups=mesh['grp'=2,'ep'=4,'tp'=4] {'ep'}, dimensions={0}, use_global_device_ids=true | all-gather | bytes 491520 | tf_op jit(solution)/shard_map/all_gather | solution.py:68
  208.6 0.2 copy.45
  208.8 0.1 copy.46
  208.9 0.8 bitcast_reduce_fusion
  209.7 0.8 fusion.4
  210.5 0.0 copy-start.15
  210.5 0.8 bitcast_reduce_fusion.1
  211.4 0.8 fusion.2
  212.2 1.0 fusion.52
  213.2 1.0 multiply_reduce_fusion.1
  214.2 0.1 multiply_convert_fusion
  214.3 0.2 copy.52
  214.5 0.8 all_to_all.20
  215.3 3.4 %all-to-all-start = ((bf16[4,96,256]{2,1,0:T(8,128)(2,1)}), bf16[4,96,256]{2,1,0:T(8,128)(2,1)S(1)}, u32[]{:S(2)}, u32[]{:S(2)}) async-start(bf16[4,96,256]{2,1,0:T(8,128)(2,1)} %all_to_all.20), calls=%async_computation | async-start | bytes 393216 | tf_op jit(solution)/shard_map/all_to_all | solution.py:110
  218.7 12.0 %reduce-scatter.2.cloned.1.call-done = bf16[512,2048]{1,0:T(8,128)(2,1)} async-done(((bf16[2048,2048]{1,0:T(8,128)(2,1)}), bf16[512,2048]{1,0:T(8,128)(2,1)}) %reduce-scatter.2.cloned.1.call-update) | async-done | bytes 2097168 | tf_op jit(solution)/shard_map/reduce_scatter | solution.py:169
  230.7 2.7 slice.36
  233.4 4.6 %all-to-all-start.2 = ((bf16[4,96,2048]{2,1,0:T(8,128)(2,1)}), bf16[4,96,2048]{2,1,0:T(8,128)(2,1)S(1)}, u32[]{:S(2)}, u32[]{:S(2)}) async-start(bf16[4,96,2048]{2,1,0:T(8,128)(2,1)} %bitcast.179), calls=%async_computation.3 | async-start | bytes 3145728 | tf_op jit(solution)/shard_map/all_to_all | solution.py:182
  238.0 0.1 copy.60
  238.2 3.7 %convolution_convert_fusion.2 = bf16[96,2048]{1,0:T(8,128)(2,1)} fusion(bf16[96,1024]{1,0:T(8,128)(2,1)S(1)} %bitcast.185, bf16[1024,2048]{1,0:T(8,128)(2,1)} %param.25), kind=kOutput, calls=%fused_computation.22 | convolution fusion | flops 402849792 | bytes 4784128 | tf_op jit(solution)/shard_map/dot_general | solution.py:111
  241.9 32.9 %all-to-all-done.2 = bf16[4,96,2048]{2,1,0:T(8,128)(2,1)S(1)} async-done(((bf16[4,96,2048]{2,1,0:T(8,128)(2,1)}), bf16[4,96,2048]{2,1,0:T(8,128)(2,1)S(1)}, u32[]{:S(2)}, u32[]{:S(2)}) %all-to-all-start.2) | async-done | bytes 1572896 | tf_op jit(solution)/shard_map/all_to_all | solution.py:182
  274.8 2.3 gather_fusion.1
  277.2 2.4 reshape.171
  279.6 3.2 %multiply_reduce_fusion = f32[128,2048]{1,0:T(8,128)S(1)} fusion(f32[128,2,2048]{2,1,0:T(2,128)S(1)} %reshape.171, f32[128,2]{1,0:T(8,128)S(1)} %copy.60), kind=kLoop, calls=%fused_computation.24 | loop fusion | flops 786432 | bytes 3146752 | tf_op jit(solution)/shard_map/reduce_sum | solution.py:186
  282.7 2.0 add_convert_fusion
  (43 shorter events, 0.3 us)
Async XLA Ops:
  7.2 123.3 %copy-start = (bf16[1,256,2048]{2,1,0:T(8,128)(2,1)S(1)}, bf16[1,256,2048]{2,1,0:T(8,128)(2,1)}, u32[]{:S(2)}) copy-start(bf16[1,256,2048]{2,1,0:T(8,128)(2,1)} %param.32) | copy-start | bytes 3145732
  14.9 9.5 %copy-start.3 = (bf16[128,2048]{1,0:T(8,128)(2,1)S(1)}, bf16[128,2048]{1,0:T(8,128)(2,1)}, u32[]{:S(2)}) copy-start(bf16[128,2048]{1,0:T(8,128)(2,1)} %param.26) | copy-start | bytes 1572868
  14.9 9.5 %copy-start.9 = (f32[2048]{0:T(1024)S(1)}, f32[2048]{0:T(1024)}, u32[]{:S(2)}) copy-start(f32[2048]{0:T(1024)} %param.27) | copy-start | bytes 24580
  18.1 43.3 %all-to-all-start.1 = ((bf16[1,4,96,2048]{3,2,0,1:T(8,128)(2,1)}), bf16[1,4,96,2048]{3,2,0,1:T(8,128)(2,1)S(1)}, u32[]{:S(2)}, u32[]{:S(2)}) async-start(bf16[1,4,96,2048]{3,2,0,1:T(8,128)(2,1)} %bitcast.182), calls=%async_computation.1 | async-start | bytes 3145728 | tf_op jit(solution)/shard_map/all_to_all | solution.py:138
  24.4 97.1 %all-gather.2.cloned.1.call-start = ((), (), s32[]{:S(2)}) async-start(), calls=%async_computation.4 | async-start | bytes 10485760 | tf_op jit(solution)/shard_map/all_gather | solution.py:142
  64.0 63.5 %copy-start.12 = (bf16[1,2048,256]{2,1,0:T(8,128)(2,1)S(1)}, bf16[1,2048,256]{2,1,0:T(8,128)(2,1)}, u32[]{:S(2)}) copy-start(bf16[1,2048,256]{2,1,0:T(8,128)(2,1)} %param.30) | copy-start | bytes 3145732
  64.0 166.7 %reduce-scatter.2.cloned.1.call-start = ((), (), s32[]{:S(2)}) async-start(), calls=%async_computation.5 | async-start | bytes 10485760 | tf_op jit(solution)/shard_map/reduce_scatter | solution.py:169
  124.9 2.6 copy-start.2
  127.5 3.1 %copy-start.13 = (bf16[1,2048,256]{2,1,0:T(8,128)(2,1)S(1)}, bf16[1,2048,256]{2,1,0:T(8,128)(2,1)}, u32[]{:S(2)}) copy-start(bf16[1,2048,256]{2,1,0:T(8,128)(2,1)} %param.31) | copy-start | bytes 3145732
  130.5 12.4 %copy-start.14 = (bf16[2048,128]{1,0:T(8,128)(2,1)S(1)}, bf16[2048,128]{1,0:T(8,128)(2,1)}, u32[]{:S(2)}) copy-start(bf16[2048,128]{1,0:T(8,128)(2,1)} %param.33) | copy-start | bytes 1572868
  157.0 0.9 copy-start.4
  157.0 20.9 %copy-start.7 = (bf16[384,128]{1,0:T(8,128)(2,1)S(1)}, bf16[384,128]{1,0:T(8,128)(2,1)}, u32[]{:S(2)}) copy-start(bf16[384,128]{1,0:T(8,128)(2,1)} %param.21) | copy-start | bytes 294916
  157.0 36.3 %copy-start.5 = (bf16[384,128]{1,0:T(8,128)(2,1)S(1)}, bf16[384,128]{1,0:T(8,128)(2,1)}, u32[]{:S(2)}) copy-start(bf16[384,128]{1,0:T(8,128)(2,1)} %param.19) | copy-start | bytes 294916
  157.0 36.5 %copy-start.8 = (bf16[384,128]{1,0:T(8,128)(2,1)S(1)}, bf16[384,128]{1,0:T(8,128)(2,1)}, u32[]{:S(2)}) copy-start(bf16[384,128]{1,0:T(8,128)(2,1)} %param.20) | copy-start | bytes 294916
  157.9 50.8 %copy-start.6 = (bf16[384,128]{1,0:T(8,128)(2,1)S(1)}, bf16[384,128]{1,0:T(8,128)(2,1)}, u32[]{:S(2)}) copy-start(bf16[384,128]{1,0:T(8,128)(2,1)} %param.18) | copy-start | bytes 294916
  210.5 1.7 copy-start.15
  213.2 1.0 copy-start.11
  214.2 23.9 %copy-start.10 = (f32[128,2]{0,1:T(2,128)S(1)}, f32[128,2]{0,1:T(2,128)}, u32[]{:S(2)}) copy-start(f32[128,2]{0,1:T(2,128)} %param.29) | copy-start | bytes 3076
  215.3 18.2 %all-to-all-start = ((bf16[4,96,256]{2,1,0:T(8,128)(2,1)}), bf16[4,96,256]{2,1,0:T(8,128)(2,1)S(1)}, u32[]{:S(2)}, u32[]{:S(2)}) async-start(bf16[4,96,256]{2,1,0:T(8,128)(2,1)} %all_to_all.20), calls=%async_computation | async-start | bytes 393216 | tf_op jit(solution)/shard_map/all_to_all | solution.py:110
  233.4 41.4 %all-to-all-start.2 = ((bf16[4,96,2048]{2,1,0:T(8,128)(2,1)}), bf16[4,96,2048]{2,1,0:T(8,128)(2,1)S(1)}, u32[]{:S(2)}, u32[]{:S(2)}) async-start(bf16[4,96,2048]{2,1,0:T(8,128)(2,1)} %bitcast.179), calls=%async_computation.3 | async-start | bytes 3145728 | tf_op jit(solution)/shard_map/all_to_all | solution.py:182
  274.8 9.9 %copy-start.1 = (bf16[1,256,2048]{2,1,0:T(8,128)(2,1)S(1)}, bf16[1,256,2048]{2,1,0:T(8,128)(2,1)}, u32[]{:S(2)}) copy-start(bf16[1,256,2048]{2,1,0:T(8,128)(2,1)} %param.32) | copy-start | bytes 3145732
Sparse Core Ops, SparseCore 0:
  64.1 57.3 all-gather.1
  157.1 73.5 reduce-scatter.1
where the time goes:
time: 292 us
  waiting for transfers between devices  138 us (47%)
  blocking collectives  50 us (17%)
  matrix products  29.3 us (10%)
  other arithmetic  22.7 us (8%)
  local copies, waits for them, and re-layouts  22.5 us (8%)
  starting transfers between devices  14.5 us (5%)
  between operations  14.4 us (5%)
    all_gather x1, waiting for transfers between devices, shards(): gathered = lax.all_gather(local_rows, 'tp', axis=0, tiled=True)  57.3 us
    all_to_all x1, waiting for transfers between devices, shards(): lax.all_to_all(outgoing, 'ep', split_axis=1, concat_axis=1, tiled=True)  36 us
    all_to_all x1, waiting for transfers between devices, shards(): lax.all_to_all(routed_back, 'ep', split_axis=0, concat_axis=0, tiled=True)  32.9 us
    all_gather x1, blocking collectives, shards(): value_piece = lax.all_gather(values, 'ep', axis=0, tiled=True)  19.7 us
    all_gather x1, blocking collectives, shards(): key_two = lax.all_gather(key_second, 'ep', axis=0, tiled=True)  15.2 us
    all_gather x1, blocking collectives, shards(): key_one = lax.all_gather(key_first, 'ep', axis=0, tiled=True)  15.1 us
    dot_general x1, matrix products, shards(): jnp.einsum('osecf,efd->osecd', hidden, expert_down, preferred_element_typ...  12.4 us
    reduce_scatter x1, waiting for transfers between devices, shards(): lax.psum_scatter(jnp.concatenate([routed_out, shared_out], axis=1).reshap...  12 us
  transfers between devices with their start and end apart: 5, of which 4 were waited for; matrix products, arithmetic and copies ran while one was open for 5% of the time, Pallas kernels for 0%

commit v1 on v0

--- a/solution.py
+++ b/solution.py
@@ -1,10 +1,16 @@
+import functools
+
 import jax
 import jax.numpy as jnp
 from jax import lax
+from jax.experimental import pallas as pl
+from jax.experimental.pallas import tpu as pltpu
 from jax.sharding import PartitionSpec as P
 
 epsilon = 1e-06
 block_limit = 1536
+lane_count = 128
+third = 32
 
 
 def key_block(total_rows, shard_rows):
@@ -30,6 +36,336 @@
         preferred_element_type=jnp.float32,
     )
     return (new_max, new_sum, accumulated * rescale[..., None] + product)
+
+
+def relay_pairs(count, width, step):
+    upward = [(z * width + t, (z + 1) * width + t) for t in range(0, width, 2) for z in range(step - 1, count - 1)]
+    downward = [(z * width + t, (z - 1) * width + t) for t in range(1, width, 2) for z in range(1, count - step + 1)]
+    return upward + downward
+
+
+def return_pairs(count, width, step):
+    downward = [(z * width + t, (z - 1) * width + t) for t in range(0, width, 2) for z in range(count - step, count)]
+    upward = [(z * width + t, (z + 1) * width + t) for t in range(1, width, 2) for z in range(step)]
+    return downward + upward
+
+
+def swap_core(value):
+    return lax.ppermute(value, "tp", [(t, t ^ 1) for t in range(lax.axis_size("tp"))])
+
+
+def swap_pair(value):
+    return lax.ppermute(value, "tp", [(t, t ^ 2) for t in range(lax.axis_size("tp"))])
+
+
+def swap_group(value):
+    return lax.ppermute(value, "grp", [(0, 1), (1, 0)])
+
+
+def silu(value):
+    return value / (1.0 + jnp.exp(-value))
+
+
+def prepare_body(own, other, route_own, route_other, gain, out):
+    rows, width = own.shape
+    for index, (block, route) in enumerate(((own, route_own), (other, route_other))):
+        wide = block[...].astype(jnp.float32)
+        scale = lax.rsqrt(jnp.mean(wide * wide, axis=-1, keepdims=True) + epsilon)
+        out[pl.ds(index * rows, rows), pl.ds(0, width)] = (wide * scale * gain[...]).astype(jnp.bfloat16)
+        lanes = lax.broadcasted_iota(jnp.int32, (rows, lane_count), 1)
+        table = route[...]
+        picks = table.shape[1] // 2
+        part = jnp.zeros((rows, lane_count), jnp.float32)
+        for pick in range(picks):
+            chosen = table[:, pick : pick + 1].astype(jnp.int32)
+            weight = table[:, picks + pick : picks + pick + 1]
+            part = part + jnp.where((lanes & (third - 1)) == chosen, weight, 0.0)
+        high = part.astype(jnp.bfloat16)
+        rest = part - high.astype(jnp.float32)
+        middle = rest.astype(jnp.bfloat16)
+        low = (rest - middle.astype(jnp.float32)).astype(jnp.bfloat16)
+        level = lanes // third
+        mixed = jnp.where(
+            level == 0,
+            high.astype(jnp.float32),
+            jnp.where(level == 1, middle.astype(jnp.float32), jnp.where(level == 2, low.astype(jnp.float32), 0.0)),
+        )
+        out[pl.ds(index * rows, rows), pl.ds(width, lane_count)] = mixed.astype(jnp.bfloat16)
+
+
+def prepare(own, other, route_own, route_other, gain):
+    rows, width = own.shape
+    return pl.pallas_call(
+        prepare_body,
+        out_shape=jax.ShapeDtypeStruct((2 * rows, width + lane_count), jnp.bfloat16),
+        cost_estimate=pl.CostEstimate(flops=8 * rows * width, bytes_accessed=8 * rows * width, transcendentals=rows),
+        name="prepare",
+    )(own, other, route_own, route_other, gain.reshape(1, width))
+
+
+def halves_body(which, gate, up, out):
+    half = gate.shape[1]
+    out[:, pl.ds(0, half)] = gate[...]
+    out[:, pl.ds(half, half)] = up[...]
+
+
+def halves(gate, up, which):
+    width, units = gate.shape
+    rows = min(512, width)
+    half = units // 2
+    return pl.pallas_call(
+        halves_body,
+        grid_spec=pltpu.PrefetchScalarGridSpec(
+            num_scalar_prefetch=1,
+            grid=(width // rows,),
+            in_specs=[
+                pl.BlockSpec((rows, half), lambda i, which: (i, which[0])),
+                pl.BlockSpec((rows, half), lambda i, which: (i, which[0])),
+            ],
+            out_specs=pl.BlockSpec((rows, units), lambda i, which: (i, 0)),
+        ),
+        out_shape=jax.ShapeDtypeStruct((width, units), jnp.bfloat16),
+        cost_estimate=pl.CostEstimate(flops=width * units, bytes_accessed=4 * width * units, transcendentals=0),
+        name="halves",
+    )(which.reshape(1), gate, up)
+
+
+def feed_forward_body(plan, block_count, weighted, *refs):
+    blocks = refs[:block_count]
+    mask = refs[block_count]
+    weight_count = plan["weights"]
+    weights = refs[block_count + 1 : block_count + 1 + weight_count]
+    outs = refs[block_count + 1 + weight_count : 2 * block_count + 1 + weight_count]
+    scratch = refs[2 * block_count + 1 + weight_count :]
+    joined_buffer, down_buffer, hidden, sems = scratch
+    width = plan["width"]
+    copies = {}
+    for number, (index, kind, start, size) in enumerate(plan["copies"]):
+        if kind == "column":
+            target = joined_buffer.at[start]
+        else:
+            target = down_buffer.at[pl.ds(start, size), :]
+        copies[index] = pltpu.make_async_copy(weights[index], target, sems.at[number])
+        copies[index].start()
+    for piece in plan["pieces"]:
+        for index in piece["needs"]:
+            copies[index].wait()
+        for number, block in enumerate(blocks):
+            rows = block.shape[0]
+            first_row = plan["rows"][number]
+            x = block[:, pl.ds(0, width)]
+            if piece["kind"] == "two":
+                gate = jnp.dot(x, joined_buffer[piece["slots"][0]], preferred_element_type=jnp.float32)
+                up = jnp.dot(x, joined_buffer[piece["slots"][1]], preferred_element_type=jnp.float32)
+            else:
+                both = jnp.dot(x, joined_buffer[piece["slots"][0]], preferred_element_type=jnp.float32)
+                units = both.shape[1] // 2
+                gate, up = both[:, :units], both[:, units:]
+            hidden[pl.ds(first_row, rows), pl.ds(piece["start"], piece["units"])] = (silu(gate) * up).astype(
+                jnp.bfloat16
+            )
+    for index in plan["downs"]:
+        copies[index].wait()
+    for number, block in enumerate(blocks):
+        rows = block.shape[0]
+        first_row = plan["rows"][number]
+        result = jnp.dot(
+            hidden[pl.ds(first_row, rows), :], down_buffer[...], preferred_element_type=jnp.float32
+        )
+        if weighted:
+            table = block[:, pl.ds(width, lane_count)].astype(jnp.float32)
+            result = result * jnp.sum(table * mask[...], axis=-1, keepdims=True)
+        outs[number][...] = result.astype(outs[number].dtype)
+
+
+def feed_forward(blocks, mask, pairs, joined, weighted, out_types, width, name):
+    weights, copies, pieces, downs = [], [], [], []
+    slot, start = 0, 0
+    for gate, up, down in pairs:
+        base = len(weights)
+        weights += [gate, up, down]
+        units = gate.shape[1]
+        copies += [(base, "column", slot, 0), (base + 1, "column", slot + 1, 0), (base + 2, "row", start, units)]
+        pieces.append({"kind": "two", "slots": (slot, slot + 1), "needs": (base, base + 1), "start": start, "units": units})
+        downs.append(base + 2)
+        slot, start = slot + 2, start + units
+    for both, down in joined:
+        base = len(weights)
+        weights += [both, down]
+        units = down.shape[0]
+        copies += [(base, "column", slot, 0), (base + 1, "row", start, units)]
+        pieces.append({"kind": "one", "slots": (slot,), "needs": (base,), "start": start, "units": units})
+        downs.append(base + 1)
+        slot, start = slot + 1, start + units
+    columns = weights[0].shape[1]
+    depth, model = weights[0].shape[0], weights[2].shape[1]
+    row_starts, total = [], 0
+    for block in blocks:
+        row_starts.append(total)
+        total += block.shape[0]
+    plan = {
+        "weights": len(weights),
+        "copies": copies,
+        "pieces": pieces,
+        "downs": downs,
+        "rows": row_starts,
+        "width": width,
+    }
+    flops = 2 * total * depth * start * 3
+    return pl.pallas_call(
+        functools.partial(feed_forward_body, plan, len(blocks), weighted),
+        in_specs=[pl.BlockSpec(memory_space=pltpu.VMEM) for _ in range(len(blocks) + 1)]
+        + [pl.BlockSpec(memory_space=pl.ANY) for _ in weights],
+        out_specs=[pl.BlockSpec(memory_space=pltpu.VMEM) for _ in blocks],
+        out_shape=[jax.ShapeDtypeStruct((block.shape[0], model), kind) for block, kind in zip(blocks, out_types)],
+        scratch_shapes=[
+            pltpu.VMEM((slot, depth, columns), jnp.bfloat16),
+            pltpu.VMEM((start, model), jnp.bfloat16),
+            pltpu.VMEM((total, start), jnp.bfloat16),
+            pltpu.SemaphoreType.DMA((len(copies),)),
+        ],
+        compiler_params=pltpu.CompilerParams(vmem_limit_bytes=48 * 1024 * 1024),
+        cost_estimate=pl.CostEstimate(
+            flops=flops, bytes_accessed=6 * depth * start + 4 * total * model, transcendentals=total * start
+        ),
+        name=name,
+    )(*blocks, mask, *weights)
+
+
+def attention(query_first, query_second, keys, head_count, lambda_head, head_gain):
+    rows, width = query_first.shape
+    size = width // head_count
+    table = jnp.concatenate(keys, axis=0)
+    values = table[:, 2 * width :]
+    value_size = values.shape[1] // head_count
+    outs = []
+    for head in range(head_count):
+        maps = []
+        for number, query in enumerate((query_first, query_second)):
+            q = query[:, head * size : (head + 1) * size]
+            k = table[:, number * width + head * size : number * width + (head + 1) * size]
+            scores = lax.dot_general(q, k, (((1,), (1,)), ((), ())), preferred_element_type=jnp.float32) * size**-0.5
+            weights = jnp.exp(scores - jnp.max(scores, axis=-1, keepdims=True))
+            total = jnp.sum(weights, axis=-1, keepdims=True)
+            product = jnp.dot(
+                weights.astype(jnp.bfloat16),
+                values[:, head * value_size : (head + 1) * value_size],
+                preferred_element_type=jnp.float32,
+            )
+            maps.append(product / total)
+        mixture = maps[0] - lambda_head[head] * maps[1]
+        outs.append(mixture * lax.rsqrt(jnp.mean(mixture * mixture, axis=-1, keepdims=True) + epsilon) * head_gain)
+    return jnp.concatenate(outs, axis=1).astype(jnp.bfloat16)
+
+
+def direct_shards(
+    query_first,
+    query_second,
+    key_first,
+    key_second,
+    values,
+    lambda_head,
+    head_gain,
+    out_weight,
+    tokens,
+    norm_gain,
+    expert_ids,
+    expert_weights,
+    expert_gate,
+    expert_up,
+    expert_down,
+    shared_gate,
+    shared_up,
+    shared_down,
+):
+    count, width_tp = lax.axis_size("ep"), lax.axis_size("tp")
+    place, group = lax.axis_index("ep"), lax.axis_index("grp")
+    heads_here = lambda_head.shape[0]
+    row_count, model_width = tokens.shape
+    gate, up, down = expert_gate[0], expert_up[0], expert_down[0]
+    units = gate.shape[1]
+
+    route = jnp.concatenate([expert_ids.astype(jnp.float32), expert_weights], axis=1)
+    pair = prepare(tokens, swap_core(tokens), route, swap_core(route), norm_gain)
+
+    sent = halves(gate, up, group)
+    sent_down = lax.dynamic_slice_in_dim(down, group * (units // 2), units // 2, axis=0)
+    near = swap_pair(sent)
+    near_down = swap_pair(sent_down)
+    far = swap_group(near)
+    far_down = swap_group(near_down)
+
+    def moved(value, step):
+        return lax.ppermute(value, ("ep", "tp"), relay_pairs(count, width_tp, step))
+
+    arrived = []
+    latest = pair
+    for step in range(1, count):
+        latest = moved(latest, step)
+        arrived.append(latest)
+
+    kv_own = jnp.concatenate([key_first, key_second, values], axis=1)
+    kv_pair = jnp.concatenate([kv_own, swap_core(kv_own)], axis=0)
+    kv_rows = kv_own.shape[0]
+    kv_mine, kv_other = [], []
+    latest = kv_pair
+    for step in range(1, count):
+        latest = moved(latest, step)
+        kv_mine.append(latest[:kv_rows])
+        kv_other.append(swap_core(latest[kv_rows:]))
+    kv_blocks = [kv_own]
+    for step in range(1, count):
+        kv_blocks.append(kv_mine[step - 1] + kv_other[count - step - 1])
+
+    lanes = jnp.arange(lane_count, dtype=jnp.int32)
+    mask = jnp.where((lanes % third == place) & (lanes < 3 * third), 1.0, 0.0).astype(jnp.float32)[None]
+    pairs = [(gate, up, down), (swap_core(gate), swap_core(up), swap_core(down))]
+    joined = [
+        (near, near_down),
+        (swap_core(near), swap_core(near_down)),
+        (far, far_down),
+        (swap_core(far), swap_core(far_down)),
+    ]
+    (last,) = feed_forward([arrived[-1]], mask, pairs, joined, True, [jnp.bfloat16], model_width, "routed_far")
+    rest_blocks = list(reversed(arrived[:-1])) + [pair[:row_count]]
+    rest = feed_forward(
+        rest_blocks,
+        mask,
+        pairs,
+        joined,
+        True,
+        [jnp.bfloat16] * (count - 2) + [jnp.float32],
+        model_width,
+        "routed_near",
+    )
+    partial = [last] + list(rest)
+    running = last
+    for step in range(1, count):
+        running = lax.ppermute(running, ("ep", "tp"), return_pairs(count, width_tp, step))
+        if step < count - 1:
+            running = (running.astype(jnp.float32) + partial[step].astype(jnp.float32)).astype(jnp.bfloat16)
+
+    shared_own = (shared_gate, shared_up, shared_down)
+    shared_near = tuple(swap_pair(piece) for piece in shared_own)
+    shared_pieces = [
+        shared_own,
+        tuple(swap_core(piece) for piece in shared_own),
+        shared_near,
+        tuple(swap_core(piece) for piece in shared_near),
+    ]
+    (shared_out,) = feed_forward(
+        [pair[:row_count]], mask, shared_pieces, [], False, [jnp.float32], model_width, "shared"
+    )
+
+    head_local = attention(query_first, query_second, kv_blocks, heads_here, lambda_head, head_gain)
+    position_heads = lax.all_to_all(head_local, "tp", split_axis=0, concat_axis=1, tiled=True)
+    mixed = jnp.dot(position_heads, out_weight, preferred_element_type=jnp.float32).astype(jnp.bfloat16)
+
+    other_half = swap_core(running[row_count:])
+    expert_out = (
+        rest[-1] + shared_out + running[:row_count].astype(jnp.float32) + other_half.astype(jnp.float32)
+    ).astype(jnp.bfloat16)
+    return (mixed, expert_out)
 
 
 def shards(
@@ -209,10 +545,26 @@
         P(None, "tp"),
         P("tp", None),
     )
-    return jax.shard_map(
-        shards,
-        mesh=mesh,
-        in_specs=placed,
-        out_specs=(P(("grp", "ep", "tp"), None), P(("grp", "ep", "tp"), None)),
-        check_vma=False,
-    )
+    sizes = dict(mesh.shape)
+
+    def chosen(*arrays):
+        experts = arrays[12].shape[0]
+        direct = (
+            sizes["grp"] == 2
+            and sizes["tp"] == 4
+            and sizes["ep"] == experts
+            and 3 <= experts <= 8
+        )
+        body = direct_shards if direct else shards
+        return mapped(body)(*arrays)
+
+    def mapped(body):
+        return jax.shard_map(
+            body,
+            mesh=mesh,
+            in_specs=placed,
+            out_specs=(P(("grp", "ep", "tp"), None), P(("grp", "ep", "tp"), None)),
+            check_vma=False,
+        )
+
+    return chosen

time: 292 us -> 183 us (0.63)
  waiting for transfers between devices: 138 us -> 48.9 us
  blocking collectives: 50 us -> 0 us
  starting transfers between devices: 14.5 us -> 64.4 us
  Pallas kernels: 0 us -> 33 us
  matrix products: 29.3 us -> 9.64 us
  other arithmetic: 22.7 us -> 9.26 us
  between operations: 14.4 us -> 1.22 us
  local copies, waits for them, and re-layouts: 22.5 us -> 15.6 us
    all_to_all x3 -> x1, waiting for transfers between devices: 68.9 us -> 0.01 us  [direct_shards(): lax.all_to_all(head_local, 'tp', split_axis=0, concat_axis=1, tiled=True)]
    ppermute x0 -> x36, starting transfers between devices: none -> 61 us  [the longest x20 35.4 us: swap_core(): lax.ppermute(value, 'tp', [(t, t ^ 1) for t in range(lax.axis_size('tp'))])]
    all_gather x1 -> x0, waiting for transfers between devices: 57.3 us -> none  [shards(): gathered = lax.all_gather(local_rows, 'tp', axis=0, tiled=True)]
    all_gather x3 -> x0, blocking collectives: 50 us -> none  [the longest x1 19.7 us: shards(): value_piece = lax.all_gather(values, 'ep', axis=0, tiled=True)]
    ppermute x0 -> x36, waiting for transfers between devices: none -> 48.9 us  [the longest x2 24.4 us: swap_group(): return lax.ppermute(value, 'grp', [(0, 1), (1, 0)])]
    pallas_call x0 -> x5, Pallas kernels: none -> 33 us  [the longest x3 26.5 us: feed_forward(): pl.pallas_call(functools.partial(feed_forward_body, plan, len(blocks), we...]
    dot_general x9, matrix products: 29.3 us -> 9.64 us  [the longest x1 3.9 us: direct_shards(): jnp.dot(position_heads, out_weight, preferred_element_type=jnp.float32)]
    reduce_scatter x1 -> x0, waiting for transfers between devices: 12 us -> none  [shards(): lax.psum_scatter(jnp.concatenate([routed_out, shared_out], axis=1).reshap...]
  transfers between devices with their start and end apart: 5 -> 37, of which waited for: 4 -> 7; matrix products, arithmetic and copies ran while one was open for 5% -> 11% of each run, Pallas kernels for 0% -> 18%
where the time goes in v1:
time: 183 us; the launch traced here: 182 us
  starting transfers between devices  64.4 us (35%)
  waiting for transfers between devices  48.9 us (27%)
  Pallas kernels  33 us (18%)
  local copies, waits for them, and re-layouts  15.6 us (9%)
  matrix products  9.64 us (5%)
  other arithmetic  9.26 us (5%)
    ppermute x20, starting transfers between devices, swap_core(): lax.ppermute(value, 'tp', [(t, t ^ 1) for t in range(lax.axis_size('tp'))])  35.4 us
    pallas_call x3, Pallas kernels, feed_forward(): pl.pallas_call(functools.partial(feed_forward_body, plan, len(blocks), we...  26.5 us
    ppermute x2, waiting for transfers between devices, swap_group(): return lax.ppermute(value, 'grp', [(0, 1), (1, 0)])  24.4 us
    ppermute x3, waiting for transfers between devices, direct_shards(): lax.ppermute(running, ('ep', 'tp'), return_pairs(count, width_tp, step))  15.5 us
    ppermute x6, starting transfers between devices, moved(): return lax.ppermute(value, ('ep', 'tp'), relay_pairs(count, width_tp, step))  13.5 us
    unnamed x84, local copies, waits for them, and re-layouts  11 us
    ppermute x5, waiting for transfers between devices, swap_pair(): lax.ppermute(value, 'tp', [(t, t ^ 2) for t in range(lax.axis_size('tp'))])  6.47 us
    ppermute x5, starting transfers between devices, swap_pair(): lax.ppermute(value, 'tp', [(t, t ^ 2) for t in range(lax.axis_size('tp'))])  5.74 us
  transfers between devices with their start and end apart: 37, of which 7 were waited for; matrix products, arithmetic and copies ran while one was open for 11% of the time, Pallas kernels for 18%

profile of v1, /device:TPU:0, one launch (start us, length us, event | category | flops | bytes accessed | tf_op | source)
XLA Modules:
  0.0 182.0 jit_solution(7152478210712423227)
XLA Ops:
  0.6 1.0 constant_dynamic-update-slice_fusion.2
  1.6 0.9 constant_dynamic-update-slice_fusion.1
  2.6 0.9 constant_dynamic-update-slice_fusion
  3.5 0.6 collective-permute-start
  4.2 1.3 collective-permute-done
  5.4 1.0 pad_maximum_fusion.1
  6.4 5.8 %collective-permute-start.1 = (bf16[768,512]{1,0:T(8,128)(2,1)}, bf16[768,512]{1,0:T(8,128)(2,1)}, u32[]{:S(2)}, u32[]{:S(2)}) collective-permute-start(bf16[768,512]{1,0:T(8,128)(2,1)} %pad_maximum_fusion.1), channel_id=1, source_target_pairs={{0,4},{4,8},{8,12},{2,6},{6,10},{10,14},{5,1},{9,5},{13,9},{7,3},{... | collective-permute-start | bytes 2359304 | tf_op jit(solution)/shard_map/ppermute | solution.py:299
  12.3 1.6 collective-permute-start.15
  13.9 3.7 %halves.1 = bf16[2048,256]{1,0:T(8,128)(2,1)} custom-call(s32[1]{0:T(128)} %bitcast.9.which, bf16[2048,256]{1,0:T(8,128)(2,1)} %bitcast.16, bf16[2048,256]{1,0:T(8,128)(2,1)} %bitcast.20), custom_call_target="tpu_custom_call" | custom-call | flops 524288 | bytes 2097152 | tf_op jit(solution)/shard_map/halves/pallas_call | solution.py:116
  17.6 0.5 collective-permute-start.14
  18.3 1.2 collective-permute-done.8.route_other
  19.6 0.6 copy-done.36
  20.2 2.8 %prepare.1 = bf16[256,2176]{1,0:T(8,128)(2,1)} custom-call(bf16[128,2048]{1,0:T(8,128)(2,1)} %own.1, bf16[128,2048]{1,0:T(8,128)(2,1)} %collective-permute-done.7.other, f32[128,4]{1,0:T(8,128)} %copy-done.35, f32[128,4]{1,0:T(8,128)} %copy-done.36, f32[1,2048]{1,0:T(1,128)} %bitcast.31), custom_call_target="tpu_custom_call" | custom-call | flops 2097152 | bytes 2097152 | tf_op jit(solution)/shard_map/prepare/pallas_call | solution.py:98
  23.0 3.7 %collective-permute-start.9 = (bf16[256,2176]{1,0:T(8,128)(2,1)}, bf16[256,2176]{1,0:T(8,128)(2,1)}, u32[]{:S(2)}, u32[]{:S(2)}) collective-permute-start(bf16[256,2176]{1,0:T(8,128)(2,1)} %prepare.1), channel_id=1, source_target_pairs={{0,4},{4,8},{8,12},{2,6},{6,10},{10,14},{5,1},{9,5},{13,9},{7,3},{... | collective-permute-start | bytes 3342344 | tf_op jit(solution)/shard_map/ppermute | solution.py:299
  26.6 0.5 collective-permute-done.15.refs_11_.refs_9_
  27.2 1.5 collective-permute-start.19
  28.7 0.7 collective-permute-start.2
  29.4 8.9 %collective-permute-done.19.refs_15_.refs_13_ = bf16[128,2048]{1,0:T(8,128)(2,1)S(1)} collective-permute-done((bf16[128,2048]{1,0:T(8,128)(2,1)S(1)}, bf16[128,2048]{1,0:T(8,128)(2,1)S(1)}, u32[]{:S(2)}, u32[]{:S(2)}) %collective-permute-start.19) | collective-permute-done | bytes 524320 | tf_op jit(solution)/shard_map/ppermute | solution.py:62
  38.4 0.8 copy-done.15
  39.7 5.9 %collective-permute-done.14.refs_10_.refs_8_ = bf16[2048,256]{1,0:T(8,128)(2,1)} collective-permute-done((bf16[2048,256]{1,0:T(8,128)(2,1)}, bf16[2048,256]{1,0:T(8,128)(2,1)}, u32[]{:S(2)}, u32[]{:S(2)}) %collective-permute-start.14) | collective-permute-done | bytes 1048608 | tf_op jit(solution)/shard_map/ppermute | solution.py:58
  45.6 1.8 collective-permute-start.18
  47.4 0.7 collective-permute-start.3
  48.1 1.7 collective-permute-start.10
  49.8 0.9 collective-permute-start.5
  50.8 0.8 collective-permute-start.13
  51.7 15.5 %collective-permute-done.18.refs_14_.refs_12_ = bf16[2048,256]{1,0:T(8,128)(2,1)} collective-permute-done((bf16[2048,256]{1,0:T(8,128)(2,1)}, bf16[2048,256]{1,0:T(8,128)(2,1)}, u32[]{:S(2)}, u32[]{:S(2)}) %collective-permute-start.18) | collective-permute-done | bytes 1048608 | tf_op jit(solution)/shard_map/ppermute | solution.py:62
  67.2 0.5 collective-permute-start.20
  68.1 0.8 slice.91
  68.9 0.8 copy-done.34
  69.7 0.5 collective-permute-start.4
  70.2 0.7 fusion.56
  70.8 1.9 %collective-permute-start.21 = (bf16[128,2048]{1,0:T(8,128)(2,1)S(1)}, bf16[128,2048]{1,0:T(8,128)(2,1)S(1)}, u32[]{:S(2)}, u32[]{:S(2)}) collective-permute-start(bf16[128,2048]{1,0:T(8,128)(2,1)S(1)} %collective-permute-done.19.refs_15_.refs_13_), channel_id=1, source_target_pairs={{0,1},{1,0},{2,3},{3,2},{4,5},{5,4},{6,7},{7,6},{8,9},{9,8},{10,11... | collective-permute-start | bytes 1572872 | tf_op jit(solution)/shard_map/ppermute | solution.py:54
  72.8 1.1 slice.102.refs_2_.refs_0_
  73.9 1.4 slice_add_fusion.1
  75.3 0.9 collective-permute-start.31
  76.2 1.3 slice_add_fusion.2
  77.5 1.6 collective-permute-start.25
  79.4 0.5 collective-permute-start.26
  80.0 1.2 copy-done.13
  81.2 1.0 copy-done.16
  82.3 13.3 %routed_near.1 = (bf16[256,2048]{1,0:T(8,128)(2,1)S(1)}, bf16[256,2048]{1,0:T(8,128)(2,1)S(1)}, f32[128,2048]{1,0:T(8,128)S(1)}) custom-call(bf16[256,2176]{1,0:T(8,128)(2,1)} %collective-permute-done.10.refs_0_, bf16[256,2176]{1,0:T(8,128)(2,1)} %collective-permute-done.9.refs_1_, bf16[128,2176]{1,0:T(8,128)(2,1)S(1)} %slice.102.refs_2_.refs_0_, ...), custom_call_target="tpu_custom_call" | custom-call | flops 8053063680 | bytes 17825792 | tf_op jit(solution)/shard_map/routed_near/pallas_call | solution.py:215
  95.6 1.6 collective-permute-start.27
  97.2 1.0 copy-done.23
  98.3 8.2 %routed_far.1 = bf16[256,2048]{1,0:T(8,128)(2,1)S(1)} custom-call(bf16[256,2176]{1,0:T(8,128)(2,1)} %copy-done.23, f32[1,128]{1,0:T(1,128)S(1)} %and_select_fusion.refs_3_.refs_1_, bf16[2048,256]{1,0:T(8,128)(2,1)S(1)} %bitcast.19, bf16[2048,256]{1,0:T(8,128)(2,1)S(1)} %bitcast.23, bf16[256,2048]{1,0:T(8,128)(2,1)} %bitcast.26, ...), custom_call_target="tpu_custom_call" | custom-call | flops 3221225472 | bytes 14680064 | tf_op jit(solution)/shard_map/routed_far/pallas_call | solution.py:215
  106.5 1.1 collective-permute-start.32
  107.7 0.6 fusion.59
  108.8 0.6 fusion.60
  109.8 0.7 collective-permute-start.33
  111.8 1.2 fusion.41
  113.0 0.6 multiply_reduce_fusion
  114.1 1.3 collective-permute-start.34
  115.4 1.2 fusion.29
  117.4 28.2 %collective-permute-start.23 = (bf16[2048,128]{1,0:T(8,128)(2,1)S(1)}, bf16[2048,128]{1,0:T(8,128)(2,1)S(1)}, u32[]{:S(2)}, u32[]{:S(2)}) collective-permute-start(bf16[2048,128]{1,0:T(8,128)(2,1)S(1)} %copy-done.6), channel_id=1, source_target_pairs={{0,1},{1,0},{2,3},{3,2},{4,5},{5,4},{6,7},{7,6},{8,9},{9,8},{10,11... | collective-permute-start | bytes 1572872 | tf_op jit(solution)/shard_map/ppermute | solution.py:54
  145.6 0.6 multiply_reduce_fusion.1
  146.9 15.4 %collective-permute-done.34 = bf16[256,2048]{1,0:T(8,128)(2,1)S(1)} collective-permute-done((bf16[256,2048]{1,0:T(8,128)(2,1)S(1)}, bf16[256,2048]{1,0:T(8,128)(2,1)S(1)}, u32[]{:S(2)}, u32[]{:S(2)}) %collective-permute-start.34) | collective-permute-done | bytes 1048608 | tf_op jit(solution)/shard_map/ppermute | solution.py:344
  162.6 0.9 slice.104
  163.5 0.8 copy-done.17
  164.7 0.7 pad_maximum_fusion.2
  165.4 3.4 %all-to-all-start = ((bf16[4,96,256]{2,1,0:T(8,128)(2,1)}), bf16[4,96,256]{2,1,0:T(8,128)(2,1)S(1)}, u32[]{:S(2)}, u32[]{:S(2)}) async-start(bf16[4,96,256]{2,1,0:T(8,128)(2,1)} %pad_maximum_fusion.2), calls=%async_computation | async-start | bytes 393216 | tf_op jit(solution)/shard_map/all_to_all | solution.py:361
  168.8 1.0 copy-done.11
  169.9 1.0 copy-done.18
  170.9 5.0 %shared.1 = f32[128,2048]{1,0:T(8,128)} custom-call(bf16[128,2176]{1,0:T(8,128)(2,1)} %copy-done.4, f32[1,128]{1,0:T(1,128)S(1)} %and_select_fusion.refs_3_.refs_1_, bf16[2048,128]{1,0:T(8,128)(2,1)S(1)} %copy-done.5, bf16[2048,128]{1,0:T(8,128)(2,1)S(1)} %copy-done.6, bf16[128,2048]{1,0:T(8,128)(2,1)S(1)} %copy-done.7, bf16[2048,128]{1,0:T(8,128)(2,1)S(1)} %copy-done.11, ...), custom_call_target="tpu_custom_call" | custom-call | flops 805306368 | bytes 7340032 | tf_op jit(solution)/shard_map/shared/pallas_call | solution.py:215
  176.0 3.9 %convolution_convert_fusion = bf16[96,2048]{1,0:T(8,128)(2,1)} fusion(bf16[96,1024]{1,0:T(8,128)(2,1)S(1)} %bitcast.27, bf16[1024,2048]{1,0:T(8,128)(2,1)} %param.25), kind=kOutput, calls=%fused_computation.8 | convolution fusion | flops 402849792 | bytes 4784128 | tf_op jit(solution)/shard_map/dot_general | solution.py:362
  179.9 2.1 %add_convert_fusion.2 = bf16[128,2048]{1,0:T(8,128)(2,1)} fusion(bf16[128,2048]{1,0:T(8,128)(2,1)} %collective-permute-done.35, f32[128,2048]{1,0:T(8,128)S(1)} %get-tuple-element.5, f32[128,2048]{1,0:T(8,128)S(1)} %copy-done.19, bf16[256,2048]{1,0:T(8,128)(2,1)S(1)} %copy-done.28), kind=kLoop, calls=%fused_computation.36 | loop fusion | flops 1572864 | bytes 3670016 | tf_op jit(solution)/shard_map/convert_element_type | solution.py:367
  (135 shorter events, 6.8 us)
Async XLA Ops:
  0.6 11.6 %copy-start.20 = (bf16[1,256,2048]{2,1,0:T(8,128)(2,1)S(1)}, bf16[1,256,2048]{2,1,0:T(8,128)(2,1)}, u32[]{:S(2)}) copy-start(bf16[1,256,2048]{2,1,0:T(8,128)(2,1)} %param.32) | copy-start | bytes 3145732
  3.5 10.3 %copy-start.21 = (bf16[384,512]{1,0:T(8,128)(2,1)}, bf16[384,512]{1,0:T(8,128)(2,1)S(1)}, u32[]{:S(2)}) copy-start(bf16[384,512]{1,0:T(8,128)(2,1)S(1)} %constant_dynamic-update-slice_fusion) | copy-start | bytes 1179652
  3.5 1.9 %collective-permute-start = (bf16[384,512]{1,0:T(8,128)(2,1)S(1)}, bf16[384,512]{1,0:T(8,128)(2,1)S(1)}, u32[]{:S(2)}, u32[]{:S(2)}) collective-permute-start(bf16[384,512]{1,0:T(8,128)(2,1)S(1)} %constant_dynamic-update-slice_fusion), channel_id=1, source_target_pairs={{0,1},{1,0},{2,3},{3,2},{4,5},{5,4},{6,7},{7,6},{8,9},{9,8},{10,11... | collective-permute-start | bytes 1179656 | tf_op jit(solution)/shard_map/ppermute | solution.py:54
  4.1 15.5 %collective-permute-start.7 = (bf16[128,2048]{1,0:T(8,128)(2,1)}, bf16[128,2048]{1,0:T(8,128)(2,1)}, u32[]{:S(2)}, u32[]{:S(2)}) collective-permute-start(bf16[128,2048]{1,0:T(8,128)(2,1)} %own.1), channel_id=1, source_target_pairs={{0,1},{1,0},{2,3},{3,2},{4,5},{5,4},{6,7},{7,6},{8,9},{9,8},{10,11... | collective-permute-start | bytes 1572872 | tf_op jit(solution)/shard_map/ppermute | solution.py:54
  6.4 11.7 %copy-start.38 = (s32[128,2]{0,1:T(2,128)S(1)}, s32[128,2]{0,1:T(2,128)}, u32[]{:S(2)}) copy-start(s32[128,2]{0,1:T(2,128)} %param.28) | copy-start | bytes 3076
  6.4 11.7 %copy-start.39 = (f32[128,2]{0,1:T(2,128)S(1)}, f32[128,2]{0,1:T(2,128)}, u32[]{:S(2)}) copy-start(f32[128,2]{0,1:T(2,128)} %param.29) | copy-start | bytes 3076
  6.4 22.3 %collective-permute-start.1 = (bf16[768,512]{1,0:T(8,128)(2,1)}, bf16[768,512]{1,0:T(8,128)(2,1)}, u32[]{:S(2)}, u32[]{:S(2)}) collective-permute-start(bf16[768,512]{1,0:T(8,128)(2,1)} %pad_maximum_fusion.1), channel_id=1, source_target_pairs={{0,4},{4,8},{8,12},{2,6},{6,10},{10,14},{5,1},{9,5},{13,9},{7,3},{... | collective-permute-start | bytes 2359304 | tf_op jit(solution)/shard_map/ppermute | solution.py:299
  12.3 14.9 %collective-permute-start.15 = (bf16[128,2048]{1,0:T(8,128)(2,1)S(1)}, bf16[128,2048]{1,0:T(8,128)(2,1)S(1)}, u32[]{:S(2)}, u32[]{:S(2)}) collective-permute-start(bf16[128,2048]{1,0:T(8,128)(2,1)S(1)} %dynamic-slice_bitcast_fusion), channel_id=1, source_target_pairs={{0,2},{1,3},{2,0},{3,1},{4,6},{5,7},{6,4},{7,5},{8,10},{9,11},{10,... | collective-permute-start | bytes 1572872 | tf_op jit(solution)/shard_map/ppermute | solution.py:58
  13.9 24.5 %copy-start = (bf16[1,2048,256]{2,1,0:T(8,128)(2,1)S(1)}, bf16[1,2048,256]{2,1,0:T(8,128)(2,1)}, u32[]{:S(2)}) copy-start(bf16[1,2048,256]{2,1,0:T(8,128)(2,1)} %param.30) | copy-start | bytes 3145732
  13.9 25.3 %copy-start.2 = (bf16[1,2048,256]{2,1,0:T(8,128)(2,1)S(1)}, bf16[1,2048,256]{2,1,0:T(8,128)(2,1)}, u32[]{:S(2)}) copy-start(bf16[1,2048,256]{2,1,0:T(8,128)(2,1)} %param.31) | copy-start | bytes 3145732
  17.5 52.6 %copy-start.37 = (f32[2]{0:T(128)S(1)}, f32[2]{0:T(128)}, u32[]{:S(2)}) copy-start(f32[2]{0:T(128)} %param.23) | copy-start | bytes 28
  17.6 28.1 %collective-permute-start.14 = (bf16[2048,256]{1,0:T(8,128)(2,1)}, bf16[2048,256]{1,0:T(8,128)(2,1)}, u32[]{:S(2)}, u32[]{:S(2)}) collective-permute-start(bf16[2048,256]{1,0:T(8,128)(2,1)} %halves.1), channel_id=1, source_target_pairs={{0,2},{1,3},{2,0},{3,1},{4,6},{5,7},{6,4},{7,5},{8,10},{9,11},{10,... | collective-permute-start | bytes 3145736 | tf_op jit(solution)/shard_map/ppermute | solution.py:58
  18.2 1.3 copy-start.35
  18.2 1.3 collective-permute-start.8
  23.0 25.1 %collective-permute-start.9 = (bf16[256,2176]{1,0:T(8,128)(2,1)}, bf16[256,2176]{1,0:T(8,128)(2,1)}, u32[]{:S(2)}, u32[]{:S(2)}) collective-permute-start(bf16[256,2176]{1,0:T(8,128)(2,1)} %prepare.1), channel_id=1, source_target_pairs={{0,4},{4,8},{8,12},{2,6},{6,10},{10,14},{5,1},{9,5},{13,9},{7,3},{... | collective-permute-start | bytes 3342344 | tf_op jit(solution)/shard_map/ppermute | solution.py:299
  27.2 23.6 %copy-start.8 = (bf16[128,2048]{1,0:T(8,128)(2,1)}, bf16[128,2048]{1,0:T(8,128)(2,1)S(1)}, u32[]{:S(2)}) copy-start(bf16[128,2048]{1,0:T(8,128)(2,1)S(1)} %collective-permute-done.15.refs_11_.refs_9_) | copy-start | bytes 1572868
  27.2 11.2 %collective-permute-start.19 = (bf16[128,2048]{1,0:T(8,128)(2,1)S(1)}, bf16[128,2048]{1,0:T(8,128)(2,1)S(1)}, u32[]{:S(2)}, u32[]{:S(2)}) collective-permute-start(bf16[128,2048]{1,0:T(8,128)(2,1)S(1)} %collective-permute-done.15.refs_11_.refs_9_), channel_id=1, source_target_pairs={{0,16},{16,0},{1,17},{17,1},{2,18},{18,2},{3,19},{19,3},{4,20},{20... | collective-permute-start | bytes 1572872 | tf_op jit(solution)/shard_map/ppermute | solution.py:62
  28.7 9.7 %collective-permute-start.17 = (bf16[128,2048]{1,0:T(8,128)(2,1)S(1)}, bf16[128,2048]{1,0:T(8,128)(2,1)S(1)}, u32[]{:S(2)}, u32[]{:S(2)}) collective-permute-start(bf16[128,2048]{1,0:T(8,128)(2,1)S(1)} %collective-permute-done.15.refs_11_.refs_9_), channel_id=1, source_target_pairs={{0,1},{1,0},{2,3},{3,2},{4,5},{5,4},{6,7},{7,6},{8,9},{9,8},{10,11... | collective-permute-start | bytes 1572872 | tf_op jit(solution)/shard_map/ppermute | solution.py:54
  28.7 18.7 %collective-permute-start.2 = (bf16[768,512]{1,0:T(8,128)(2,1)}, bf16[768,512]{1,0:T(8,128)(2,1)S(1)}, u32[]{:S(2)}, u32[]{:S(2)}) collective-permute-start(bf16[768,512]{1,0:T(8,128)(2,1)} %collective-permute-done.1), channel_id=1, source_target_pairs={{4,8},{8,12},{6,10},{10,14},{5,1},{9,5},{7,3},{11,7},{20,24},{24,2... | collective-permute-start | bytes 2359304 | tf_op jit(solution)/shard_map/ppermute | solution.py:299
  38.3 39.1 %copy-start.12 = (bf16[128,2048]{1,0:T(8,128)(2,1)}, bf16[128,2048]{1,0:T(8,128)(2,1)S(1)}, u32[]{:S(2)}) copy-start(bf16[128,2048]{1,0:T(8,128)(2,1)S(1)} %collective-permute-done.19.refs_15_.refs_13_) | copy-start | bytes 1572868
  38.3 11.5 %collective-permute-start.11 = (bf16[2048,256]{1,0:T(8,128)(2,1)S(1)}, bf16[2048,256]{1,0:T(8,128)(2,1)S(1)}, u32[]{:S(2)}, u32[]{:S(2)}) collective-permute-start(bf16[2048,256]{1,0:T(8,128)(2,1)S(1)} %bitcast.18), channel_id=1, source_target_pairs={{0,1},{1,0},{2,3},{3,2},{4,5},{5,4},{6,7},{7,6},{8,9},{9,8},{10,11... | collective-permute-start | bytes 3145736 | tf_op jit(solution)/shard_map/ppermute | solution.py:54
  39.2 11.5 %collective-permute-start.12 = (bf16[2048,256]{1,0:T(8,128)(2,1)S(1)}, bf16[2048,256]{1,0:T(8,128)(2,1)S(1)}, u32[]{:S(2)}, u32[]{:S(2)}) collective-permute-start(bf16[2048,256]{1,0:T(8,128)(2,1)S(1)} %bitcast.22), channel_id=1, source_target_pairs={{0,1},{1,0},{2,3},{3,2},{4,5},{5,4},{6,7},{7,6},{8,9},{9,8},{10,11... | collective-permute-start | bytes 3145736 | tf_op jit(solution)/shard_map/ppermute | solution.py:54
  45.6 21.6 %collective-permute-start.18 = (bf16[2048,256]{1,0:T(8,128)(2,1)}, bf16[2048,256]{1,0:T(8,128)(2,1)}, u32[]{:S(2)}, u32[]{:S(2)}) collective-permute-start(bf16[2048,256]{1,0:T(8,128)(2,1)} %collective-permute-done.14.refs_10_.refs_8_), channel_id=1, source_target_pairs={{0,16},{16,0},{1,17},{17,1},{2,18},{18,2},{3,19},{19,3},{4,20},{20... | collective-permute-start | bytes 3145736 | tf_op jit(solution)/shard_map/ppermute | solution.py:62
  47.4 21.5 %copy-start.31 = (bf16[768,512]{1,0:T(8,128)(2,1)}, bf16[768,512]{1,0:T(8,128)(2,1)S(1)}, u32[]{:S(2)}) copy-start(bf16[768,512]{1,0:T(8,128)(2,1)S(1)} %collective-permute-done.2) | copy-start | bytes 2359300
  47.4 19.9 %collective-permute-start.3 = (bf16[768,512]{1,0:T(8,128)(2,1)S(1)}, bf16[768,512]{1,0:T(8,128)(2,1)S(1)}, u32[]{:S(2)}, u32[]{:S(2)}) collective-permute-start(bf16[768,512]{1,0:T(8,128)(2,1)S(1)} %collective-permute-done.2), channel_id=1, source_target_pairs={{8,12},{10,14},{5,1},{7,3},{24,28},{26,30},{21,17},{23,19}} | collective-permute-start | bytes 2359304 | tf_op jit(solution)/shard_map/ppermute | solution.py:299
  48.1 22.7 %collective-permute-start.10 = (bf16[256,2176]{1,0:T(8,128)(2,1)}, bf16[256,2176]{1,0:T(8,128)(2,1)}, u32[]{:S(2)}, u32[]{:S(2)}) collective-permute-start(bf16[256,2176]{1,0:T(8,128)(2,1)} %collective-permute-done.9.refs_1_), channel_id=1, source_target_pairs={{4,8},{8,12},{6,10},{10,14},{5,1},{9,5},{7,3},{11,7},{20,24},{24,2... | collective-permute-start | bytes 3342344 | tf_op jit(solution)/shard_map/ppermute | solution.py:299
  49.8 19.1 %collective-permute-start.5 = (bf16[384,512]{1,0:T(8,128)(2,1)S(1)}, bf16[384,512]{1,0:T(8,128)(2,1)S(1)}, u32[]{:S(2)}, u32[]{:S(2)}) collective-permute-start(bf16[384,512]{1,0:T(8,128)(2,1)S(1)} %slice.93), channel_id=1, source_target_pairs={{0,1},{1,0},{2,3},{3,2},{4,5},{5,4},{6,7},{7,6},{8,9},{9,8},{10,11... | collective-permute-start | bytes 1179656 | tf_op jit(solution)/shard_map/ppermute | solution.py:54
  50.8 26.7 %copy-start.5 = (bf16[2048,128]{1,0:T(8,128)(2,1)S(1)}, bf16[2048,128]{1,0:T(8,128)(2,1)}, u32[]{:S(2)}) copy-start(bf16[2048,128]{1,0:T(8,128)(2,1)} %refs_2_.1) | copy-start | bytes 1572868
  50.8 28.6 %copy-start.6 = (bf16[2048,128]{1,0:T(8,128)(2,1)S(1)}, bf16[2048,128]{1,0:T(8,128)(2,1)}, u32[]{:S(2)}) copy-start(bf16[2048,128]{1,0:T(8,128)(2,1)} %refs_3_.1) | copy-start | bytes 1572868
  50.8 26.7 %collective-permute-start.13 = (bf16[256,2048]{1,0:T(8,128)(2,1)}, bf16[256,2048]{1,0:T(8,128)(2,1)S(1)}, u32[]{:S(2)}, u32[]{:S(2)}) collective-permute-start(bf16[256,2048]{1,0:T(8,128)(2,1)} %bitcast.24), channel_id=1, source_target_pairs={{0,1},{1,0},{2,3},{3,2},{4,5},{5,4},{6,7},{7,6},{8,9},{9,8},{10,11... | collective-permute-start | bytes 3145736 | tf_op jit(solution)/shard_map/ppermute | solution.py:54
  67.2 12.1 %collective-permute-start.16 = (bf16[2048,256]{1,0:T(8,128)(2,1)}, bf16[2048,256]{1,0:T(8,128)(2,1)}, u32[]{:S(2)}, u32[]{:S(2)}) collective-permute-start(bf16[2048,256]{1,0:T(8,128)(2,1)} %collective-permute-done.14.refs_10_.refs_8_), channel_id=1, source_target_pairs={{0,1},{1,0},{2,3},{3,2},{4,5},{5,4},{6,7},{7,6},{8,9},{9,8},{10,11... | collective-permute-start | bytes 3145736 | tf_op jit(solution)/shard_map/ppermute | solution.py:54
  67.2 12.7 %collective-permute-start.20 = (bf16[2048,256]{1,0:T(8,128)(2,1)}, bf16[2048,256]{1,0:T(8,128)(2,1)}, u32[]{:S(2)}, u32[]{:S(2)}) collective-permute-start(bf16[2048,256]{1,0:T(8,128)(2,1)} %collective-permute-done.18.refs_14_.refs_12_), channel_id=1, source_target_pairs={{0,1},{1,0},{2,3},{3,2},{4,5},{5,4},{6,7},{7,6},{8,9},{9,8},{10,11... | collective-permute-start | bytes 3145736 | tf_op jit(solution)/shard_map/ppermute | solution.py:54
  69.7 5.6 %collective-permute-start.4 = (bf16[384,512]{1,0:T(8,128)(2,1)}, bf16[384,512]{1,0:T(8,128)(2,1)}, u32[]{:S(2)}, u32[]{:S(2)}) collective-permute-start(bf16[384,512]{1,0:T(8,128)(2,1)} %slice.91), channel_id=1, source_target_pairs={{0,1},{1,0},{2,3},{3,2},{4,5},{5,4},{6,7},{7,6},{8,9},{9,8},{10,11... | collective-permute-start | bytes 1179656 | tf_op jit(solution)/shard_map/ppermute | solution.py:54
  70.8 9.2 %copy-start.9 = (bf16[128,2048]{1,0:T(8,128)(2,1)S(1)}, bf16[128,2048]{1,0:T(8,128)(2,1)}, u32[]{:S(2)}) copy-start(bf16[128,2048]{1,0:T(8,128)(2,1)} %copy-done.8) | copy-start | bytes 1572868
  70.8 8.2 %collective-permute-start.21 = (bf16[128,2048]{1,0:T(8,128)(2,1)S(1)}, bf16[128,2048]{1,0:T(8,128)(2,1)S(1)}, u32[]{:S(2)}, u32[]{:S(2)}) collective-permute-start(bf16[128,2048]{1,0:T(8,128)(2,1)S(1)} %collective-permute-done.19.refs_15_.refs_13_), channel_id=1, source_target_pairs={{0,1},{1,0},{2,3},{3,2},{4,5},{5,4},{6,7},{7,6},{8,9},{9,8},{10,11... | collective-permute-start | bytes 1572872 | tf_op jit(solution)/shard_map/ppermute | solution.py:54
  73.9 21.7 %copy-start.4 = (bf16[128,2176]{1,0:T(8,128)(2,1)}, bf16[128,2176]{1,0:T(8,128)(2,1)S(1)}, u32[]{:S(2)}) copy-start(bf16[128,2176]{1,0:T(8,128)(2,1)S(1)} %slice.102.refs_2_.refs_0_) | copy-start | bytes 1671172
  75.3 22.0 %collective-permute-start.31 = (bf16[256,2176]{1,0:T(8,128)(2,1)}, bf16[256,2176]{1,0:T(8,128)(2,1)S(1)}, u32[]{:S(2)}, u32[]{:S(2)}) collective-permute-start(bf16[256,2176]{1,0:T(8,128)(2,1)} %collective-permute-done.10.refs_0_), channel_id=1, source_target_pairs={{8,12},{10,14},{5,1},{7,3},{24,28},{26,30},{21,17},{23,19}} | collective-permute-start | bytes 3342344 | tf_op jit(solution)/shard_map/ppermute | solution.py:299
  77.5 2.4 %copy-start.26 = (bf16[256,2048]{1,0:T(8,128)(2,1)}, bf16[256,2048]{1,0:T(8,128)(2,1)S(1)}, u32[]{:S(2)}) copy-start(bf16[256,2048]{1,0:T(8,128)(2,1)S(1)} %collective-permute-done.13.refs_9_.refs_7_) | copy-start | bytes 3145732
  77.5 39.9 %collective-permute-start.25 = (bf16[2048,128]{1,0:T(8,128)(2,1)S(1)}, bf16[2048,128]{1,0:T(8,128)(2,1)}, u32[]{:S(2)}, u32[]{:S(2)}) collective-permute-start(bf16[2048,128]{1,0:T(8,128)(2,1)S(1)} %copy-done.5), channel_id=1, source_target_pairs={{0,2},{1,3},{2,0},{3,1},{4,6},{5,7},{6,4},{7,5},{8,10},{9,11},{10,... | collective-permute-start | bytes 1572872 | tf_op jit(solution)/shard_map/ppermute | solution.py:58
  79.1 67.7 %collective-permute-start.22 = (bf16[2048,128]{1,0:T(8,128)(2,1)S(1)}, bf16[2048,128]{1,0:T(8,128)(2,1)S(1)}, u32[]{:S(2)}, u32[]{:S(2)}) collective-permute-start(bf16[2048,128]{1,0:T(8,128)(2,1)S(1)} %copy-done.5), channel_id=1, source_target_pairs={{0,1},{1,0},{2,3},{3,2},{4,5},{5,4},{6,7},{7,6},{8,9},{9,8},{10,11... | collective-permute-start | bytes 1572872 | tf_op jit(solution)/shard_map/ppermute | solution.py:54
  79.4 66.9 %collective-permute-start.26 = (bf16[2048,128]{1,0:T(8,128)(2,1)S(1)}, bf16[2048,128]{1,0:T(8,128)(2,1)}, u32[]{:S(2)}, u32[]{:S(2)}) collective-permute-start(bf16[2048,128]{1,0:T(8,128)(2,1)S(1)} %copy-done.6), channel_id=1, source_target_pairs={{0,2},{1,3},{2,0},{3,1},{4,6},{5,7},{6,4},{7,5},{8,10},{9,11},{10,... | collective-permute-start | bytes 1572872 | tf_op jit(solution)/shard_map/ppermute | solution.py:58
  79.9 15.7 %copy-start.7 = (bf16[128,2048]{1,0:T(8,128)(2,1)S(1)}, bf16[128,2048]{1,0:T(8,128)(2,1)}, u32[]{:S(2)}) copy-start(bf16[128,2048]{1,0:T(8,128)(2,1)} %refs_4_.1) | copy-start | bytes 1572868
  79.9 18.4 %copy-start.1 = (bf16[1,2048,256]{2,1,0:T(8,128)(2,1)S(1)}, bf16[1,2048,256]{2,1,0:T(8,128)(2,1)}, u32[]{:S(2)}) copy-start(bf16[1,2048,256]{2,1,0:T(8,128)(2,1)} %param.30) | copy-start | bytes 3145732
  79.9 18.4 %copy-start.3 = (bf16[1,2048,256]{2,1,0:T(8,128)(2,1)S(1)}, bf16[1,2048,256]{2,1,0:T(8,128)(2,1)}, u32[]{:S(2)}) copy-start(bf16[1,2048,256]{2,1,0:T(8,128)(2,1)} %param.31) | copy-start | bytes 3145732
  79.9 15.7 %collective-permute-start.6 = (bf16[384,512]{1,0:T(8,128)(2,1)S(1)}, bf16[384,512]{1,0:T(8,128)(2,1)S(1)}, u32[]{:S(2)}, u32[]{:S(2)}) collective-permute-start(bf16[384,512]{1,0:T(8,128)(2,1)S(1)} %get-tuple-element.9), channel_id=1, source_target_pairs={{0,1},{1,0},{2,3},{3,2},{4,5},{5,4},{6,7},{7,6},{8,9},{9,8},{10,11... | collective-permute-start | bytes 1179656 | tf_op jit(solution)/shard_map/ppermute | solution.py:54
  82.3 14.9 %copy-start.30 = (bf16[768,512]{1,0:T(8,128)(2,1)S(1)}, bf16[768,512]{1,0:T(8,128)(2,1)}, u32[]{:S(2)}) copy-start(bf16[768,512]{1,0:T(8,128)(2,1)} %copy-done.29) | copy-start | bytes 2359300
  82.3 16.0 %copy-start.14 = (bf16[128,2048]{1,0:T(8,128)(2,1)S(1)}, bf16[128,2048]{1,0:T(8,128)(2,1)}, u32[]{:S(2)}) copy-start(bf16[128,2048]{1,0:T(8,128)(2,1)} %copy-done.12) | copy-start | bytes 1572868
  95.6 50.7 %collective-permute-start.27 = (bf16[128,2048]{1,0:T(8,128)(2,1)S(1)}, bf16[128,2048]{1,0:T(8,128)(2,1)S(1)}, u32[]{:S(2)}, u32[]{:S(2)}) collective-permute-start(bf16[128,2048]{1,0:T(8,128)(2,1)S(1)} %copy-done.7), channel_id=1, source_target_pairs={{0,2},{1,3},{2,0},{3,1},{4,6},{5,7},{6,4},{7,5},{8,10},{9,11},{10,... | collective-permute-start | bytes 1572872 | tf_op jit(solution)/shard_map/ppermute | solution.py:58
  97.2 10.4 %copy-start.22 = (bf16[384,512]{1,0:T(8,128)(2,1)S(1)}, bf16[384,512]{1,0:T(8,128)(2,1)}, u32[]{:S(2)}) copy-start(bf16[384,512]{1,0:T(8,128)(2,1)} %copy-done.21) | copy-start | bytes 1179652
  106.5 2.9 %collective-permute-start.32 = (bf16[256,2048]{1,0:T(8,128)(2,1)S(1)}, bf16[256,2048]{1,0:T(8,128)(2,1)S(1)}, u32[]{:S(2)}, u32[]{:S(2)}) collective-permute-start(bf16[256,2048]{1,0:T(8,128)(2,1)S(1)} %routed_far.1), channel_id=1, source_target_pairs={{12,8},{14,10},{1,5},{3,7},{28,24},{30,26},{17,21},{19,23}} | collective-permute-start | bytes 3145736 | tf_op jit(solution)/shard_map/ppermute | solution.py:344
  109.8 3.8 %collective-permute-start.33 = (bf16[256,2048]{1,0:T(8,128)(2,1)S(1)}, bf16[256,2048]{1,0:T(8,128)(2,1)S(1)}, u32[]{:S(2)}, u32[]{:S(2)}) collective-permute-start(bf16[256,2048]{1,0:T(8,128)(2,1)S(1)} %add_convert_fusion.1), channel_id=1, source_target_pairs={{8,4},{12,8},{10,6},{14,10},{1,5},{5,9},{3,7},{7,11},{24,20},{28,2... | collective-permute-start | bytes 3145736 | tf_op jit(solution)/shard_map/ppermute | solution.py:344
  114.1 48.3 %collective-permute-start.34 = (bf16[256,2048]{1,0:T(8,128)(2,1)S(1)}, bf16[256,2048]{1,0:T(8,128)(2,1)S(1)}, u32[]{:S(2)}, u32[]{:S(2)}) collective-permute-start(bf16[256,2048]{1,0:T(8,128)(2,1)S(1)} %add_convert_fusion), channel_id=1, source_target_pairs={{4,0},{8,4},{12,8},{6,2},{10,6},{14,10},{1,5},{5,9},{9,13},{3,7},{... | collective-permute-start | bytes 3145736 | tf_op jit(solution)/shard_map/ppermute | solution.py:344
  117.0 45.4 %copy-start.40 = (f32[128]{0:T(128)S(1)}, f32[128]{0:T(128)}, u32[]{:S(2)}) copy-start(f32[128]{0:T(128)} %param.24) | copy-start | bytes 1540
  117.4 46.1 %collective-permute-start.23 = (bf16[2048,128]{1,0:T(8,128)(2,1)S(1)}, bf16[2048,128]{1,0:T(8,128)(2,1)S(1)}, u32[]{:S(2)}, u32[]{:S(2)}) collective-permute-start(bf16[2048,128]{1,0:T(8,128)(2,1)S(1)} %copy-done.6), channel_id=1, source_target_pairs={{0,1},{1,0},{2,3},{3,2},{4,5},{5,4},{6,7},{7,6},{8,9},{9,8},{10,11... | collective-permute-start | bytes 1572872 | tf_op jit(solution)/shard_map/ppermute | solution.py:54
  146.2 22.6 %collective-permute-start.24 = (bf16[128,2048]{1,0:T(8,128)(2,1)S(1)}, bf16[128,2048]{1,0:T(8,128)(2,1)}, u32[]{:S(2)}, u32[]{:S(2)}) collective-permute-start(bf16[128,2048]{1,0:T(8,128)(2,1)S(1)} %copy-done.7), channel_id=1, source_target_pairs={{0,1},{1,0},{2,3},{3,2},{4,5},{5,4},{6,7},{7,6},{8,9},{9,8},{10,11... | collective-permute-start | bytes 1572872 | tf_op jit(solution)/shard_map/ppermute | solution.py:54
  146.3 22.5 %collective-permute-start.28 = (bf16[2048,128]{1,0:T(8,128)(2,1)}, bf16[2048,128]{1,0:T(8,128)(2,1)}, u32[]{:S(2)}, u32[]{:S(2)}) collective-permute-start(bf16[2048,128]{1,0:T(8,128)(2,1)} %collective-permute-done.25.refs_8_), channel_id=1, source_target_pairs={{0,1},{1,0},{2,3},{3,2},{4,5},{5,4},{6,7},{7,6},{8,9},{9,8},{10,11... | collective-permute-start | bytes 1572872 | tf_op jit(solution)/shard_map/ppermute | solution.py:54
  146.8 16.7 %copy-start.10 = (bf16[2048,128]{1,0:T(8,128)(2,1)}, bf16[2048,128]{1,0:T(8,128)(2,1)S(1)}, u32[]{:S(2)}) copy-start(bf16[2048,128]{1,0:T(8,128)(2,1)S(1)} %collective-permute-done.22.refs_5_) | copy-start | bytes 1572868
  146.8 22.0 %collective-permute-start.29 = (bf16[2048,128]{1,0:T(8,128)(2,1)}, bf16[2048,128]{1,0:T(8,128)(2,1)}, u32[]{:S(2)}, u32[]{:S(2)}) collective-permute-start(bf16[2048,128]{1,0:T(8,128)(2,1)} %collective-permute-done.26.refs_9_), channel_id=1, source_target_pairs={{0,1},{1,0},{2,3},{3,2},{4,5},{5,4},{6,7},{7,6},{8,9},{9,8},{10,11... | collective-permute-start | bytes 1572872 | tf_op jit(solution)/shard_map/ppermute | solution.py:54
  162.4 2.4 %copy-start.27 = (bf16[256,2048]{1,0:T(8,128)(2,1)}, bf16[256,2048]{1,0:T(8,128)(2,1)S(1)}, u32[]{:S(2)}) copy-start(bf16[256,2048]{1,0:T(8,128)(2,1)S(1)} %collective-permute-done.34) | copy-start | bytes 3145732
  162.4 6.5 %collective-permute-start.30 = (bf16[128,2048]{1,0:T(8,128)(2,1)S(1)}, bf16[128,2048]{1,0:T(8,128)(2,1)}, u32[]{:S(2)}, u32[]{:S(2)}) collective-permute-start(bf16[128,2048]{1,0:T(8,128)(2,1)S(1)} %collective-permute-done.27.refs_10_), channel_id=1, source_target_pairs={{0,1},{1,0},{2,3},{3,2},{4,5},{5,4},{6,7},{7,6},{8,9},{9,8},{10,11... | collective-permute-start | bytes 1572872 | tf_op jit(solution)/shard_map/ppermute | solution.py:54
  164.3 15.6 %collective-permute-start.35 = (bf16[128,2048]{1,0:T(8,128)(2,1)}, bf16[128,2048]{1,0:T(8,128)(2,1)}, u32[]{:S(2)}, u32[]{:S(2)}) collective-permute-start(bf16[128,2048]{1,0:T(8,128)(2,1)} %slice.104), channel_id=1, source_target_pairs={{0,1},{1,0},{2,3},{3,2},{4,5},{5,4},{6,7},{7,6},{8,9},{9,8},{10,11... | collective-permute-start | bytes 1572872 | tf_op jit(solution)/shard_map/ppermute | solution.py:54
  165.4 10.5 %all-to-all-start = ((bf16[4,96,256]{2,1,0:T(8,128)(2,1)}), bf16[4,96,256]{2,1,0:T(8,128)(2,1)S(1)}, u32[]{:S(2)}, u32[]{:S(2)}) async-start(bf16[4,96,256]{2,1,0:T(8,128)(2,1)} %pad_maximum_fusion.2), calls=%async_computation | async-start | bytes 393216 | tf_op jit(solution)/shard_map/all_to_all | solution.py:361
  175.9 3.9 %copy-start.19 = (f32[128,2048]{1,0:T(8,128)S(1)}, f32[128,2048]{1,0:T(8,128)}, u32[]{:S(2)}) copy-start(f32[128,2048]{1,0:T(8,128)} %shared.1) | copy-start | bytes 3145732
  175.9 3.9 %copy-start.28 = (bf16[256,2048]{1,0:T(8,128)(2,1)S(1)}, bf16[256,2048]{1,0:T(8,128)(2,1)}, u32[]{:S(2)}) copy-start(bf16[256,2048]{1,0:T(8,128)(2,1)} %copy-done.27) | copy-start | bytes 3145732
  (14 other events, 13.6 us)
